TPU v7x, 32 devices: a whole 2x2x4 slice. The times are simulated.
32 devices in a mesh: sp: 16 (over z, y, x), tp: 2 (over core).
Axes of the slice: x: 2, y: 2, z: 4, core: 2. Of those that a mesh axis runs over, the one named last changes fastest.
Arguments:
- stream: bfloat16 [6144, 2048], P('sp'), may hold values from -40 to 40
- query_rows: bfloat16 [6144, 1024], P('sp', 'tp'), may hold values from -10 to 10
- key_rows: bfloat16 [6144, 256], P('sp'), may hold values from -10 to 10
- value_rows: bfloat16 [6144, 256], P('sp'), may hold values from -6 to 6
- doc_ids: int32 [6144], P('sp'), may hold values from 0 to 7, never falling along the last dimension, each value on 1 to 1536 neighbouring positions
- sink_logit: float32 [8], P('tp'), may hold values from 2 to 7
- out_weight: bfloat16 [1024, 2048], P('tp'), may hold values from -1.5 to 1.5
- norm_gain: float32 [2048], replicated, may hold values from 0.1 to 1.9
- gate_weight: bfloat16 [2048, 5632], P('sp', 'tp'), may hold values from -0.125 to 0.125
- up_weight: bfloat16 [2048, 5632], P('sp', 'tp'), may hold values from -0.125 to 0.125
- down_weight: bfloat16 [5632, 2048], P('tp', 'sp'), may hold values from -0.078125 to 0.078125
Outputs:
- mixed_out: bfloat16 [6144, 2048], P('sp')
Inputs may be any that keep to these rules, and one draw needn't show every extreme that they name: `doc_ids`: document numbers never fall along the sequence; each document has 1 to 1536 positions.
All inputs are finite; a program needn't handle non-finite values.
Results may differ from a plain program's by a relative error of at most 0.009.
Values may be sent and summed in bfloat16 or wider, within the bound.
A program may use at most 128 MiB of HBM per device.

v0:
```python
import jax
import jax.numpy as jnp
from jax import lax
from jax.sharding import PartitionSpec as P

HEADS = 8
KVH = 2
HD = 128
WIN = 128


norm_eps = 1e-06
masked_low = -1e30


def extended(value, sides, width):
    for axis, dim in sides:
        peers, length = (lax.axis_size(axis), value.shape[dim])
        up = [(i, (i + 1) % peers) for i in range(peers - 1)]
        down = [(j, i) for i, j in up]
        last = lax.slice_in_dim(value, length - width, length, axis=dim)
        initial = lax.slice_in_dim(value, 0, width, axis=dim)
        before = lax.ppermute(last, axis, up)
        after = lax.ppermute(initial, axis, down)
        value = jnp.concatenate([before, value, after], axis=dim)
    return value


def per_device(
    stream,
    query_rows,
    key_rows,
    value_rows,
    doc_ids,
    sink_logit,
    out_weight,
    norm_gain,
    gate_weight,
    up_weight,
    down_weight,
):
    row_count = stream.shape[0]
    heads_here = query_rows.shape[1] // HD
    group_share = HEADS // KVH
    groups_here = max(1, heads_here // group_share)
    per_group = heads_here // groups_here
    tp_place = lax.axis_index("tp")
    group_first = tp_place * heads_here // group_share
    keys_here = lax.dynamic_slice_in_dim(key_rows, group_first * HD, groups_here * HD, 1)
    values_here = lax.dynamic_slice_in_dim(value_rows, group_first * HD, groups_here * HD, 1)
    keys_wide, values_wide, docs_wide = (
        extended(keys_here, (("sp", 0),), WIN),
        extended(values_here, (("sp", 0),), WIN),
        extended(doc_ids, (("sp", 0),), WIN),
    )
    seq_offset = lax.axis_index("sp") * row_count
    seq_total = row_count * lax.axis_size("sp")
    query_pos = seq_offset + jnp.arange(row_count, dtype=jnp.int32)
    key_pos = seq_offset - WIN + jnp.arange(row_count + 2 * WIN, dtype=jnp.int32)
    allowed = (
        (jnp.abs(query_pos[:, None] - key_pos[None, :]) <= WIN)
        & (key_pos[None, :] >= 0)
        & (key_pos[None, :] < seq_total)
        & (doc_ids[:, None] == docs_wide[None, :])
    )
    queries = query_rows.reshape(row_count, groups_here, per_group, HD)
    keys_grid = keys_wide.reshape(row_count + 2 * WIN, groups_here, HD)
    values_grid = values_wide.reshape(row_count + 2 * WIN, groups_here, HD)
    scores = jnp.einsum(
        "qgrd,kgd->grqk", queries, keys_grid, preferred_element_type=jnp.float32
    ) * HD ** (-0.5)
    masked = jnp.where(allowed[None, None], scores, masked_low)
    sinks = sink_logit.reshape(groups_here, per_group, 1, 1)
    peak = jnp.maximum(jnp.max(masked, axis=-1, keepdims=True), sinks)
    lifted = jnp.where(allowed[None, None], jnp.exp(masked - peak), 0.0)
    denom = jnp.sum(lifted, axis=-1, keepdims=True) + jnp.exp(sinks - peak)
    probs = (lifted / denom).astype(jnp.bfloat16)
    attended = jnp.einsum("grqk,kgd->qgrd", probs, values_grid, preferred_element_type=jnp.float32)
    attended = attended.astype(jnp.bfloat16).reshape(row_count, heads_here * HD)
    partial_value = jnp.dot(attended, out_weight, preferred_element_type=jnp.float32)
    branch = lax.psum(partial_value.astype(jnp.bfloat16), "tp")
    carried = (stream.astype(jnp.float32) + branch.astype(jnp.float32)).astype(jnp.bfloat16)
    carried_f = carried.astype(jnp.float32)
    normed = (
        carried_f
        * lax.rsqrt(jnp.mean(carried_f * carried_f, axis=1, keepdims=True) + norm_eps)
        * norm_gain[None, :]
    ).astype(jnp.bfloat16)

    def add_rows(weight_rows):
        return jnp.dot(normed, weight_rows, preferred_element_type=jnp.float32)

    gate_acc = add_rows(lax.all_gather(gate_weight, "sp", axis=0, tiled=True))
    up_acc = add_rows(lax.all_gather(up_weight, "sp", axis=0, tiled=True))
    hidden = (jax.nn.silu(gate_acc) * up_acc).astype(jnp.bfloat16)
    terms = jnp.dot(
        hidden,
        lax.all_gather(down_weight, "sp", axis=1, tiled=True),
        preferred_element_type=jnp.float32,
    )
    feed = lax.psum(terms.astype(jnp.bfloat16), "tp")
    return (carried_f + 0.5 * feed.astype(jnp.float32)).astype(jnp.bfloat16)


def solution(mesh):
    in_specs = (
        P("sp", None),
        P("sp", "tp"),
        P("sp", None),
        P("sp", None),
        P("sp"),
        P("tp"),
        P("tp", None),
        P(),
        P("sp", "tp"),
        P("sp", "tp"),
        P("tp", "sp"),
    )
    out_specs = P("sp", None)
    return jax.shard_map(
        per_device, mesh=mesh, in_specs=in_specs, out_specs=out_specs, check_vma=False
    )
```

profile of v0, /device:TPU:0, one launch (start us, length us, event | category | flops | bytes accessed | tf_op | source)
XLA Modules:
  0.0 561.7 jit_solution(12022949672108720570)
XLA Ops:
  7.4 0.0 copy-start
  7.4 0.0 copy-start.1
  7.4 0.0 all-reduce.3.cloned.1.call-start
  7.4 0.9 fusion.38
  8.3 4.9 collective-permute-start.4
  13.2 1.3 collective-permute-start.5
  14.5 0.8 fusion.40
  15.2 4.5 collective-permute-start.2
  19.8 1.3 collective-permute-start.3
  21.1 1.0 constant_dynamic-slice_fusion.1
  22.1 0.1 copy.16
  22.2 4.9 collective-permute-start
  27.2 0.0 collective-permute-done.2
  27.2 1.3 collective-permute-start.1
  28.5 0.0 collective-permute-done.3
  28.5 0.7 pad_add_fusion
  29.2 1.4 fusion.14
  30.6 0.0 collective-permute-done.4
  30.6 0.0 collective-permute-done.5
  30.6 1.8 fusion.1
  32.4 0.0 copy-done.1
  32.4 0.1 broadcast_maximum_fusion
  32.5 1.0 fusion.6
  33.5 0.1 exponential_add_fusion
  33.6 0.0 collective-permute-done
  33.6 0.3 collective-permute-done.1
  33.9 1.5 fusion.9
  35.4 0.0 copy-done
  35.4 2.2 convolution_convert_fusion.1
  37.6 0.0 copy-start.2
  37.6 0.0 all-reduce.3.cloned.1.call-update
  37.6 0.0 all-gather.4.cloned.1.call-start
  37.6 0.5 all-gather.4.cloned.1.call-update
  38.2 0.0 all-gather.6.cloned.1.call-start
  38.2 0.5 all-gather.6.cloned.1.call-update
  38.8 0.0 all-gather.8.cloned.1.call-start
  38.8 0.5 all-gather.8.cloned.1.call-update
  39.3 0.2 all-reduce.5.cloned.1.call-start
  39.6 23.8 %all-reduce.3.cloned.1.call-done = bf16[384,2048]{1,0:T(8,128)(2,1)} async-done(((bf16[384,2048]{1,0:T(8,128)(2,1)}), bf16[384,2048]{1,0:T(8,128)(2,1)}) %all-reduce.3.cloned.1.call-update) | async-done | bytes 1572880 | tf_op jit(solution)/shard_map/psum | solution.py:81
  63.3 3.6 fusion.2
  66.9 120.3 %all-gather.4.cloned.1.call-done = bf16[2048,2816]{1,0:T(8,128)(2,1)} async-done(((bf16[128,2816]{1,0:T(8,128)(2,1)}), bf16[2048,2816]{1,0:T(8,128)(2,1)}) %all-gather.4.cloned.1.call-update) | async-done | bytes 11534352 | tf_op jit(solution)/shard_map/all_gather | solution.py:93
  187.2 0.0 copy-done.2
  187.2 11.5 %fusion.17 = f32[384,2816]{1,0:T(8,128)} fusion(bf16[2048,2816]{1,0:T(8,128)(2,1)} %all-gather.4.cloned.1.call-done, bf16[384,2048]{1,0:T(8,128)(2,1)} %get-tuple-element.6, f32[2048]{0:T(1024)S(1)} %copy-done.2, f32[384]{0:T(512)S(1)} %add_rsqrt_fusion), kind=kOutput, calls=%fused_computation.24 | convolution fusion | flops 4432330752 | bytes 17442304 | tf_op jit(solution)/shard_map/dot_general | solution.py:91
  198.8 130.5 %all-gather.6.cloned.1.call-done = bf16[2048,2816]{1,0:T(8,128)(2,1)} async-done(((bf16[128,2816]{1,0:T(8,128)(2,1)}), bf16[2048,2816]{1,0:T(8,128)(2,1)}) %all-gather.6.cloned.1.call-update) | async-done | bytes 11534352 | tf_op jit(solution)/shard_map/all_gather | solution.py:94
  329.3 182.7 %all-gather.8.cloned.1.call-done = bf16[2816,2048]{1,0:T(8,128)(2,1)} async-done(((bf16[2816,128]{1,0:T(8,128)(2,1)}), bf16[2816,2048]{1,0:T(8,128)(2,1)}) %all-gather.8.cloned.1.call-update) | async-done | bytes 11534352 | tf_op jit(solution)/shard_map/all_gather | solution.py:98
  511.9 19.8 %convolution_convert_fusion = bf16[384,2048]{1,0:T(8,128)(2,1)} fusion(bf16[2816,2048]{1,0:T(8,128)(2,1)} %all-gather.8.cloned.1.call-done, bf16[2048,2816]{1,0:T(8,128)(2,1)} %all-gather.6.cloned.1.call-done, f32[384,2816]{1,0:T(8,128)} %fusion.17, bf16[384,2048]{1,0:T(8,128)(2,1)} %get-tuple-element.6, f32[2048]{0:T(1024)S(1)} %copy-done.2, ...), kind=kOutput, calls=%fused_computation.14 | convolution fusion | flops 8868790272 | bytes 30549504 | tf_op jit(solution)/shard_map/dot_general | solution.py:96
  531.7 0.0 all-reduce.5.cloned.1.call-update
  531.7 18.7 %all-reduce.5.cloned.1.call-done = bf16[384,2048]{1,0:T(8,128)(2,1)} async-done(((bf16[384,2048]{1,0:T(8,128)(2,1)}), bf16[384,2048]{1,0:T(8,128)(2,1)}) %all-reduce.5.cloned.1.call-update) | async-done | bytes 1572880 | tf_op jit(solution)/shard_map/psum | solution.py:101
  550.5 3.7 fusion.5
  (5 shorter events, 0.0 us)
Async XLA Ops:
  7.4 28.0 %copy-start = (bf16[512,2048]{1,0:T(8,128)(2,1)S(1)}, bf16[512,2048]{1,0:T(8,128)(2,1)}, u32[]{:S(2)}) copy-start(bf16[512,2048]{1,0:T(8,128)(2,1)} %param.17) | copy-start | bytes 6291460
  7.4 25.1 %copy-start.1 = (f32[4]{0:T(128)S(1)}, f32[4]{0:T(128)}, u32[]{:S(2)}) copy-start(f32[4]{0:T(128)} %param.16) | copy-start | bytes 52
  7.4 56.0 %all-reduce.3.cloned.1.call-start = ((), (), s32[]{:S(2)}) async-start(), calls=%async_computation | async-start | bytes 3145728 | tf_op jit(solution)/shard_map/psum | solution.py:81
  8.3 22.3 %collective-permute-start.4 = (bf16[128,128]{1,0:T(8,128)(2,1)S(1)}, bf16[128,128]{1,0:T(8,128)(2,1)S(1)}, u32[]{:S(2)}, u32[]{:S(2)}) collective-permute-start(bf16[128,128]{1,0:T(8,128)(2,1)S(1)} %get-tuple-element.7), channel_id=1, source_target_pairs={{0,2},{2,4},{4,6},{6,8},{8,10},{10,12},{12,14},{14,16},{16,18},{18... | collective-permute-start | bytes 98312 | tf_op jit(solution)/shard_map/ppermute | solution.py:23
  13.2 17.4 %collective-permute-start.5 = (bf16[128,128]{1,0:T(8,128)(2,1)S(1)}, bf16[128,128]{1,0:T(8,128)(2,1)S(1)}, u32[]{:S(2)}, u32[]{:S(2)}) collective-permute-start(bf16[128,128]{1,0:T(8,128)(2,1)S(1)} %get-tuple-element.8), channel_id=1, source_target_pairs={{2,0},{4,2},{6,4},{8,6},{10,8},{12,10},{14,12},{16,14},{18,16},{20... | collective-permute-start | bytes 98312 | tf_op jit(solution)/shard_map/ppermute | solution.py:24
  15.2 11.9 %collective-permute-start.2 = (s32[128]{0:T(128)S(1)}, s32[128]{0:T(128)S(1)}, u32[]{:S(2)}, u32[]{:S(2)}) collective-permute-start(s32[128]{0:T(128)S(1)} %get-tuple-element.11), channel_id=1, source_target_pairs={{0,2},{2,4},{4,6},{6,8},{8,10},{10,12},{12,14},{14,16},{16,18},{18... | collective-permute-start | bytes 1544 | tf_op jit(solution)/shard_map/ppermute | solution.py:23
  19.8 8.7 %collective-permute-start.3 = (s32[128]{0:T(128)S(1)}, s32[128]{0:T(128)S(1)}, u32[]{:S(2)}, u32[]{:S(2)}) collective-permute-start(s32[128]{0:T(128)S(1)} %get-tuple-element.12), channel_id=1, source_target_pairs={{2,0},{4,2},{6,4},{8,6},{10,8},{12,10},{14,12},{16,14},{18,16},{20... | collective-permute-start | bytes 1544 | tf_op jit(solution)/shard_map/ppermute | solution.py:24
  22.2 11.4 %collective-permute-start = (bf16[128,128]{0,1:T(8,128)(2,1)S(1)}, bf16[128,128]{0,1:T(8,128)(2,1)S(1)}, u32[]{:S(2)}, u32[]{:S(2)}) collective-permute-start(bf16[128,128]{0,1:T(8,128)(2,1)S(1)} %get-tuple-element.9), channel_id=1, source_target_pairs={{0,2},{2,4},{4,6},{6,8},{8,10},{10,12},{12,14},{14,16},{16,18},{18... | collective-permute-start | bytes 98312 | tf_op jit(solution)/shard_map/ppermute | solution.py:23
  27.2 6.7 %collective-permute-start.1 = (bf16[128,128]{0,1:T(8,128)(2,1)S(1)}, bf16[128,128]{0,1:T(8,128)(2,1)S(1)}, u32[]{:S(2)}, u32[]{:S(2)}) collective-permute-start(bf16[128,128]{0,1:T(8,128)(2,1)S(1)} %get-tuple-element.10), channel_id=1, source_target_pairs={{2,0},{4,2},{6,4},{8,6},{10,8},{12,10},{14,12},{16,14},{18,16},{20... | collective-permute-start | bytes 98312 | tf_op jit(solution)/shard_map/ppermute | solution.py:24
  37.6 149.7 %copy-start.2 = (f32[2048]{0:T(1024)S(1)}, f32[2048]{0:T(1024)}, u32[]{:S(2)}) copy-start(f32[2048]{0:T(1024)} %param.18) | copy-start | bytes 24580
  37.6 149.7 %all-gather.4.cloned.1.call-start = ((), (), s32[]{:S(2)}) async-start(), calls=%async_computation.1 | async-start | bytes 12255232 | tf_op jit(solution)/shard_map/all_gather | solution.py:93
  38.2 291.1 %all-gather.6.cloned.1.call-start = ((), (), s32[]{:S(2)}) async-start(), calls=%async_computation.2 | async-start | bytes 12255232 | tf_op jit(solution)/shard_map/all_gather | solution.py:94
  38.8 473.2 %all-gather.8.cloned.1.call-start = ((), (), s32[]{:S(2)}) async-start(), calls=%async_computation.3 | async-start | bytes 12255232 | tf_op jit(solution)/shard_map/all_gather | solution.py:98
  39.3 511.1 %all-reduce.5.cloned.1.call-start = ((), (), s32[]{:S(2)}) async-start(), calls=%async_computation.4 | async-start | bytes 3145728 | tf_op jit(solution)/shard_map/psum | solution.py:101
Sparse Core Ops, SparseCore 0:
  37.7 25.5 all-reduce.2
  531.9 18.5 all-reduce.4
Sparse Core Ops, SparseCore 1:
  40.8 146.4 all-gather.3
  189.9 139.3 all-gather.5
  331.8 180.0 all-gather.7
where the time goes:
time: 562 us
  waiting for transfers between devices  478 us (85%)
  matrix products  36.8 us (7%)
  starting transfers between devices  18.6 us (3%)
  between operations  15.2 us (3%)
  other arithmetic  10.5 us (2%)
    all_gather x1, waiting for transfers between devices, per_device(): lax.all_gather(down_weight, 'sp', axis=1, tiled=True)  183 us
    all_gather x1, waiting for transfers between devices, per_device(): up_acc = add_rows(lax.all_gather(up_weight, 'sp', axis=0, tiled=True))  130 us
    all_gather x1, waiting for transfers between devices, per_device(): gate_acc = add_rows(lax.all_gather(gate_weight, 'sp', axis=0, tiled=True))  120 us
    psum x1, waiting for transfers between devices, per_device(): branch = lax.psum(partial_value.astype(jnp.bfloat16), 'tp')  23.8 us
    dot_general x1, matrix products, per_device(): jnp.dot(hidden, lax.all_gather(down_weight, 'sp', axis=1, tiled=True), pr...  19.8 us
    psum x1, waiting for transfers between devices, per_device(): feed = lax.psum(terms.astype(jnp.bfloat16), 'tp')  18.7 us
    ppermute x3, starting transfers between devices, extended(): before = lax.ppermute(last, axis, up)  14.3 us
    dot_general x1, matrix products, add_rows(): return jnp.dot(normed, weight_rows, preferred_element_type=jnp.float32)  11.5 us
  transfers between devices with their start and end apart: 11, of which 6 were waited for; matrix products, arithmetic and copies ran while one was open for 4% of the time, Pallas kernels for 0%

commit v1 on v0

v1 whole, which is shorter than its diff:
```python
import jax
import jax.numpy as jnp
from jax import lax
from jax.sharding import Mesh, PartitionSpec as P

HEADS = 8
KVH = 2
HD = 128
WIN = 128

norm_eps = 1e-06
masked_low = -1e30
SP = ("sa", "sb")


def halo(value, width):
    peers = lax.axis_size(SP)
    length = value.shape[0]
    up = [(i, i + 1) for i in range(peers - 1)]
    down = [(j, i) for i, j in up]
    before = lax.ppermute(value[length - width :], SP, up)
    after = lax.ppermute(value[:width], SP, down)
    return jnp.concatenate([before, value, after], axis=0)


def exchange(blocks):
    peers = lax.axis_size("sa")
    here = lax.axis_index("sa")
    got = [lax.dynamic_index_in_dim(blocks, here, 0, keepdims=True)]
    for k in range(1, peers):
        out = lax.dynamic_index_in_dim(blocks, lax.rem(here + k, peers), 0, keepdims=True)
        got.append(lax.ppermute(out, "sa", [(i, (i + k) % peers) for i in range(peers)]))
    ring = got[::-1]
    both = jnp.concatenate(ring + ring, axis=0)
    return lax.dynamic_slice_in_dim(both, peers - 1 - here, peers, 0)


def per_device(
    stream,
    query_rows,
    key_rows,
    value_rows,
    doc_ids,
    sink_logit,
    out_weight,
    norm_gain,
    gate_weight,
    up_weight,
    down_weight,
):
    row_count, width = stream.shape
    n_a, n_b, n_tp = lax.axis_size("sa"), lax.axis_size("sb"), lax.axis_size("tp")
    depth, hidden_here = gate_weight.shape
    share = hidden_here // n_a
    tp_place = lax.axis_index("tp")
    sp_place = lax.axis_index(SP)

    def shares(w):
        return w.reshape(depth, n_a, share).transpose(1, 0, 2)

    gate_up = exchange(jnp.concatenate([shares(gate_weight), shares(up_weight)], axis=2))
    gate_up = gate_up.reshape(n_a * depth, 2 * share)
    gate_up = lax.all_gather(gate_up, "sb", axis=0, tiled=True)
    down_mine = exchange(down_weight.reshape(n_a, share, depth))
    down_mine = down_mine.transpose(0, 2, 1).reshape(n_a * depth, share)

    heads_here = query_rows.shape[1] // HD
    group_share = HEADS // KVH
    groups_here = max(1, heads_here // group_share)
    per_group = heads_here // groups_here
    group_first = tp_place * heads_here // group_share
    keys_here = lax.dynamic_slice_in_dim(key_rows, group_first * HD, groups_here * HD, 1)
    values_here = lax.dynamic_slice_in_dim(value_rows, group_first * HD, groups_here * HD, 1)
    docs_col = jnp.broadcast_to(doc_ids.astype(jnp.bfloat16)[:, None], (row_count, HD))
    packed = halo(jnp.concatenate([keys_here, values_here, docs_col], axis=1), WIN)
    span = groups_here * HD
    keys_wide, values_wide = packed[:, :span], packed[:, span : 2 * span]
    docs_wide = packed[:, 2 * span].astype(jnp.int32)
    seq_offset = sp_place * row_count
    seq_total = row_count * n_a * n_b
    query_pos = seq_offset + jnp.arange(row_count, dtype=jnp.int32)
    key_pos = seq_offset - WIN + jnp.arange(row_count + 2 * WIN, dtype=jnp.int32)
    allowed = (
        (jnp.abs(query_pos[:, None] - key_pos[None, :]) <= WIN)
        & (key_pos[None, :] >= 0)
        & (key_pos[None, :] < seq_total)
        & (doc_ids[:, None] == docs_wide[None, :])
    )
    queries = query_rows.reshape(row_count, groups_here, per_group, HD)
    keys_grid = keys_wide.reshape(row_count + 2 * WIN, groups_here, HD)
    values_grid = values_wide.reshape(row_count + 2 * WIN, groups_here, HD)
    scores = jnp.einsum(
        "qgrd,kgd->grqk", queries, keys_grid, preferred_element_type=jnp.float32
    ) * HD ** (-0.5)
    masked = jnp.where(allowed[None, None], scores, masked_low)
    sinks = sink_logit.reshape(groups_here, per_group, 1, 1)
    peak = jnp.maximum(jnp.max(masked, axis=-1, keepdims=True), sinks)
    lifted = jnp.where(allowed[None, None], jnp.exp(masked - peak), 0.0)
    denom = jnp.sum(lifted, axis=-1, keepdims=True) + jnp.exp(sinks - peak)
    probs = (lifted / denom).astype(jnp.bfloat16)
    attended = jnp.einsum("grqk,kgd->qgrd", probs, values_grid, preferred_element_type=jnp.float32)
    attended = attended.astype(jnp.bfloat16).reshape(row_count, heads_here * HD)
    partial_value = jnp.dot(attended, out_weight, preferred_element_type=jnp.float32)

    rows_mine = row_count // n_tp
    branch = lax.psum_scatter(
        partial_value.astype(jnp.bfloat16), "tp", scatter_dimension=0, tiled=True
    )
    stream_mine = lax.dynamic_slice_in_dim(stream, tp_place * rows_mine, rows_mine, 0)
    carried = (stream_mine.astype(jnp.float32) + branch.astype(jnp.float32)).astype(jnp.bfloat16)
    carried_f = carried.astype(jnp.float32)
    normed = (
        carried_f
        * lax.rsqrt(jnp.mean(carried_f * carried_f, axis=1, keepdims=True) + norm_eps)
        * norm_gain[None, :]
    ).astype(jnp.bfloat16)
    normed = normed.reshape(rows_mine, n_a, n_b, depth).transpose(0, 2, 1, 3).reshape(rows_mine, width)
    rows_all = lax.all_gather(normed, ("sa", "tp"), axis=0, tiled=True)
    down_mine, _ = lax.optimization_barrier((down_mine, normed))
    down_all = lax.all_gather(down_mine, "sb", axis=0, tiled=True)

    gate_acc = jnp.dot(rows_all, gate_up[:, :share], preferred_element_type=jnp.float32)
    up_acc = jnp.dot(rows_all, gate_up[:, share:], preferred_element_type=jnp.float32)
    hidden = (jax.nn.silu(gate_acc) * up_acc).astype(jnp.bfloat16)
    terms = lax.dot_general(
        hidden, down_all, (((1,), (1,)), ((), ())), preferred_element_type=jnp.float32
    )
    feed = lax.psum_scatter(
        terms.astype(jnp.bfloat16), ("sa", "tp"), scatter_dimension=0, tiled=True
    )
    feed = feed.reshape(rows_mine, n_b, n_a, depth).transpose(0, 2, 1, 3).reshape(rows_mine, width)
    mixed = (carried_f + 0.5 * feed.astype(jnp.float32)).astype(jnp.bfloat16)
    return lax.all_gather(mixed, "tp", axis=0, tiled=True)


def solution(mesh):
    n_sp, n_tp = mesh.shape["sp"], mesh.shape["tp"]
    n_a = 4 if n_sp % 4 == 0 else 1
    fine = Mesh(mesh.devices.reshape(n_a, n_sp // n_a, n_tp), ("sa", "sb", "tp"))
    in_specs = (
        P(SP, None),
        P(SP, "tp"),
        P(SP, None),
        P(SP, None),
        P(SP),
        P("tp"),
        P("tp", None),
        P(),
        P(SP, "tp"),
        P(SP, "tp"),
        P("tp", SP),
    )
    return jax.shard_map(
        per_device, mesh=fine, in_specs=in_specs, out_specs=P(SP, None), check_vma=False
    )
```

time: 562 us -> 362 us (0.64)
  waiting for transfers between devices: 478 us -> 253 us
  local copies, waits for them, and re-layouts: 2.81 us -> 28.9 us
    all_gather x3 -> x4, waiting for transfers between devices: 433 us -> 122 us  [the longest x1 66.1 us: per_device(): rows_all = lax.all_gather(normed, ('sa', 'tp'), axis=0, tiled=True)]
    reduce_scatter x0 -> x2, waiting for transfers between devices: none -> 69.5 us  [the longest x1 69.4 us: per_device(): lax.psum_scatter(terms.astype(jnp.bfloat16), ('sa', 'tp'), scatter_dimens...]
    ppermute x6 -> x8, waiting for transfers between devices: 0.34 us -> 61.7 us  [the longest x6 56.5 us: exchange(): lax.ppermute(out, 'sa', [(i, (i + k) % peers) for i in range(peers)])]
    psum x2 -> x0, waiting for transfers between devices: 42.5 us -> none  [the longest x1 23.8 us: per_device(): branch = lax.psum(partial_value.astype(jnp.bfloat16), 'tp')]
    mul x0 -> x3, local copies, waits for them, and re-layouts: none -> 8.13 us  [per_device(): mixed = (carried_f + 0.5 * feed.astype(jnp.float32)).astype(jnp.bfloat16)]
    concatenate x0 -> x1, local copies, waits for them, and re-layouts: none -> 7.4 us  [exchange(): both = jnp.concatenate(ring + ring, axis=0)]
    unnamed x7 -> x28, local copies, waits for them, and re-layouts: 0.13 us -> 6.59 us
    ppermute x6 -> x8, starting transfers between devices: 18.2 us -> 15.5 us  [the longest x6 9.32 us: exchange(): lax.ppermute(out, 'sa', [(i, (i + k) % peers) for i in range(peers)])]
  transfers between devices with their start and end apart: 11 -> 14, of which waited for: 6 -> 11; matrix products, arithmetic and copies ran while one was open for 4% -> 8% of each run, Pallas kernels for 0% -> 0%
where the time goes in v1:
time: 362 us; the launch traced here: 361 us
  waiting for transfers between devices  253 us (70%)
  matrix products  37.1 us (10%)
  local copies, waits for them, and re-layouts  28.9 us (8%)
  starting transfers between devices  16.1 us (4%)
  between operations  15.4 us (4%)
  other arithmetic  10.4 us (3%)
    reduce_scatter x1, waiting for transfers between devices, per_device(): lax.psum_scatter(terms.astype(jnp.bfloat16), ('sa', 'tp'), scatter_dimens...  69.4 us
    all_gather x1, waiting for transfers between devices, per_device(): rows_all = lax.all_gather(normed, ('sa', 'tp'), axis=0, tiled=True)  66.1 us
    ppermute x6, waiting for transfers between devices, exchange(): lax.ppermute(out, 'sa', [(i, (i + k) % peers) for i in range(peers)])  56.5 us
    all_gather x1, waiting for transfers between devices, per_device(): down_all = lax.all_gather(down_mine, 'sb', axis=0, tiled=True)  31.3 us
    dot_general x1, matrix products, per_device(): lax.dot_general(hidden, down_all, (((1,), (1,)), ((), ())), preferred_ele...  21.3 us
    all_gather x1, waiting for transfers between devices, per_device(): gate_up = lax.all_gather(gate_up, 'sb', axis=0, tiled=True)  16.2 us
    dot_general x1, matrix products, per_device(): jnp.dot(rows_all, gate_up[:, :share], preferred_element_type=jnp.float32)  10.5 us
    ppermute x6, starting transfers between devices, exchange(): lax.ppermute(out, 'sa', [(i, (i + k) % peers) for i in range(peers)])  9.32 us
  transfers between devices with their start and end apart: 14, of which 11 were waited for; matrix products, arithmetic and copies ran while one was open for 8% of the time, Pallas kernels for 0%

profile of v1, /device:TPU:0, one launch (start us, length us, event | category | flops | bytes accessed | tf_op | source)
XLA Modules:
  0.0 361.3 jit_solution(14193642974242643932)
XLA Ops:
  7.4 0.8 convert_element_type.59
  8.2 1.0 constant_dynamic-slice_fusion.6
  9.2 0.1 broadcast_in_dim.20
  9.3 4.9 %collective-permute-start = (bf16[128,384]{1,0:T(8,128)(2,1)S(1)}, bf16[128,384]{1,0:T(8,128)(2,1)S(1)}, u32[]{:S(2)}, u32[]{:S(2)}) collective-permute-start(bf16[128,384]{1,0:T(8,128)(2,1)S(1)} %get-tuple-element.16), channel_id=1, source_target_pairs={{0,2},{2,4},{4,6},{6,8},{8,10},{10,12},{12,14},{14,16},{16,18},{18... | collective-permute-start | bytes 294920 | tf_op jit(solution)/shard_map/ppermute | solution.py:21
  14.2 1.3 collective-permute-start.1
  15.6 0.8 collective-permute-done
  16.4 4.3 %collective-permute-done.1 = bf16[128,384]{1,0:T(8,128)(2,1)S(1)} collective-permute-done((bf16[128,384]{1,0:T(8,128)(2,1)S(1)}, bf16[128,384]{1,0:T(8,128)(2,1)S(1)}, u32[]{:S(2)}, u32[]{:S(2)}) %collective-permute-start.1) | collective-permute-done | bytes 98336 | tf_op jit(solution)/shard_map/ppermute | solution.py:22
  20.7 0.1 pad_maximum_fusion
  20.8 0.2 convert_reduce_fusion
  21.0 1.4 fusion.16
  22.4 1.8 fusion
  24.2 0.1 broadcast_maximum_fusion
  24.3 1.0 fusion.4
  25.3 0.1 exponential_add_fusion
  25.3 1.5 fusion.11
  26.9 2.2 convolution_convert_fusion.1
  29.0 0.0 all-gather.7.cloned.1.call-start
  29.1 0.3 copy.20
  29.5 0.3 copy.21
  29.8 0.8 fusion.23
  30.7 3.6 collective-permute-start.2
  34.3 1.0 collective-permute-start.4
  35.3 8.2 %collective-permute-done.2 = bf16[1,128,1408]{1,2,0:T(8,128)(2,1)S(1)} collective-permute-done((bf16[1,128,1408]{1,2,0:T(8,128)(2,1)}, bf16[1,128,1408]{1,2,0:T(8,128)(2,1)S(1)}, u32[]{:S(2)}, u32[]{:S(2)}) %collective-permute-start.2) | collective-permute-done | bytes 360480 | tf_op jit(solution)/shard_map/ppermute | solution.py:32
  43.5 20.6 %collective-permute-done.3 = bf16[1,128,1408]{1,2,0:T(8,128)(2,1)S(1)} collective-permute-done((bf16[1,128,1408]{1,2,0:T(8,128)(2,1)S(1)}, bf16[1,128,1408]{1,2,0:T(8,128)(2,1)S(1)}, u32[]{:S(2)}, u32[]{:S(2)}) %collective-permute-start.3) | collective-permute-done | bytes 360480 | tf_op jit(solution)/shard_map/ppermute | solution.py:32
  64.2 0.1 constant_dynamic-update-slice_fusion.4
  64.4 0.1 constant_dynamic-update-slice_fusion
  64.5 0.1 constant_dynamic-slice_fusion.5
  64.6 1.6 copy.22
  66.2 0.0 all-gather.5.cloned.1.call-start
  66.2 1.7 fusion.7
  68.0 0.3 fusion.9
  68.2 0.6 reshape.241
  68.8 0.4 copy.47
  69.2 1.5 reshape.242
  70.7 0.0 all-gather.9.cloned.1.call-start
  70.8 1.2 constant_dynamic-slice_fusion.1
  72.0 0.3 copy.31
  72.3 0.1 collective-permute-start.5
  72.4 0.3 copy.32
  72.7 2.6 collective-permute-start.6
  75.3 0.3 copy.33
  75.5 2.1 collective-permute-start.7
  77.6 0.3 copy.34
  77.9 3.3 collective-permute-done.5
  81.2 24.5 %collective-permute-done.6 = bf16[1,704,128]{2,0,1:T(2,128)(2,1)S(1)} collective-permute-done((bf16[1,704,128]{2,0,1:T(2,128)(2,1)S(1)}, bf16[1,704,128]{2,0,1:T(2,128)(2,1)S(1)}, u32[]{:S(2)}, u32[]{:S(2)}) %collective-permute-start.6) | collective-permute-done | bytes 180256 | tf_op jit(solution)/shard_map/ppermute | solution.py:32
  105.7 0.7 copy-done.2
  106.5 7.4 %concatenate.19 = bf16[8,704,128]{2,0,1:T(8,128)(2,1)S(1)} concatenate(bf16[1,704,128]{2,0,1:T(2,128)(2,1)S(1)} %collective-permute-done.5, bf16[1,704,128]{2,0,1:T(2,128)(2,1)} %copy-done.2, bf16[1,704,128]{2,0,1:T(2,128)(2,1)} %collective-permute-done.7, bf16[1,704,128]{2,0,1:T(2,128)(2,1)S(1)} %copy.34, bf16[1,704,128]{2,0,1:T(2,128)(2,1)S(1)} %collective-permute-done.5, ...), dimensions={0} | concatenate | bytes 2883584 | tf_op jit(solution)/shard_map/concatenate | solution.py:34
  113.9 0.4 constant_dynamic-slice_fusion
  114.3 1.0 copy.48
  115.3 0.2 reduce-scatter.5.cloned.1.call-start
  115.5 16.2 %all-gather.7.cloned.1.call-done = bf16[2048,1408]{1,0:T(8,128)(2,1)} async-done(((bf16[512,1408]{1,0:T(8,128)(2,1)}), bf16[2048,1408]{1,0:T(8,128)(2,1)}) %all-gather.7.cloned.1.call-update) | async-done | bytes 5767184 | tf_op jit(solution)/shard_map/all_gather | solution.py:63
  131.7 66.1 %all-gather.5.cloned.1.call-done = bf16[1536,2048]{1,0:T(8,128)(2,1)} async-done(((bf16[192,2048]{1,0:T(8,128)(2,1)}), bf16[1536,2048]{1,0:T(8,128)(2,1)}) %all-gather.5.cloned.1.call-update) | async-done | bytes 6291472 | tf_op jit(solution)/shard_map/all_gather | solution.py:118
  197.8 10.5 %fusion.2 = f32[1536,704]{0,1:T(8,128)} fusion(bf16[1536,2048]{1,0:T(8,128)(2,1)} %all-gather.5.cloned.1.call-done, bf16[2048,1408]{1,0:T(8,128)(2,1)} %all-gather.7.cloned.1.call-done), kind=kOutput, calls=%fused_computation.7 | convolution fusion | flops 4429185024 | bytes 13762560 | tf_op jit(solution)/shard_map/dot_general | solution.py:122
  208.3 31.3 %all-gather.9.cloned.1.call-done = bf16[2048,704]{0,1:T(8,128)(2,1)} async-done(((bf16[512,704]{0,1:T(8,128)(2,1)}), bf16[2048,704]{0,1:T(8,128)(2,1)}) %all-gather.9.cloned.1.call-update) | async-done | bytes 2883600 | tf_op jit(solution)/shard_map/all_gather | solution.py:120
  239.6 21.3 %convolution_convert_fusion = bf16[1536,2048]{1,0:T(8,128)(2,1)} fusion(bf16[2048,704]{0,1:T(8,128)(2,1)} %all-gather.9.cloned.1.call-done, f32[1536,704]{0,1:T(8,128)} %fusion.2, bf16[1536,2048]{1,0:T(8,128)(2,1)} %all-gather.5.cloned.1.call-done, bf16[2048,1408]{1,0:T(8,128)(2,1)} %all-gather.7.cloned.1.call-done), kind=kOutput, calls=%fused_computation | convolution fusion | flops 8868003840 | bytes 22937600 | tf_op jit(solution)/shard_map/dot_general | solution.py:125
  260.9 0.3 all-gather.11.cloned.1.call-start
  261.1 69.4 %reduce-scatter.5.cloned.1.call-done = bf16[192,2048]{1,0:T(8,128)(2,1)} async-done(((bf16[1536,2048]{1,0:T(8,128)(2,1)}), bf16[192,2048]{1,0:T(8,128)(2,1)}) %reduce-scatter.5.cloned.1.call-update) | async-done | bytes 786448 | tf_op jit(solution)/shard_map/reduce_scatter | solution.py:128
  330.6 1.3 convert_multiply_fusion.2
  331.9 2.2 mul.87
  334.1 3.0 copy.46
  337.1 2.9 mul.89
  340.0 2.5 fusion.10
  342.5 8.5 %all-gather.11.cloned.1.call-done = bf16[384,2048]{1,0:T(8,128)(2,1)} async-done(((bf16[192,2048]{1,0:T(8,128)(2,1)}), bf16[384,2048]{1,0:T(8,128)(2,1)}) %all-gather.11.cloned.1.call-update) | async-done | bytes 1572880 | tf_op jit(solution)/shard_map/all_gather | solution.py:133
  351.0 2.7 copy.57
  (35 shorter events, 0.5 us)
Async XLA Ops:
  7.4 19.5 %copy-start = (bf16[512,2048]{1,0:T(8,128)(2,1)S(1)}, bf16[512,2048]{1,0:T(8,128)(2,1)}, u32[]{:S(2)}) copy-start(bf16[512,2048]{1,0:T(8,128)(2,1)} %param.17) | copy-start | bytes 6291460
  7.4 58.9 %reduce-scatter.3.cloned.1.call-start = ((), (), s32[]{:S(2)}) async-start(), calls=%async_computation.2 | async-start | bytes 2359296 | tf_op jit(solution)/shard_map/reduce_scatter | solution.py:106
  9.3 7.1 %collective-permute-start = (bf16[128,384]{1,0:T(8,128)(2,1)S(1)}, bf16[128,384]{1,0:T(8,128)(2,1)S(1)}, u32[]{:S(2)}, u32[]{:S(2)}) collective-permute-start(bf16[128,384]{1,0:T(8,128)(2,1)S(1)} %get-tuple-element.16), channel_id=1, source_target_pairs={{0,2},{2,4},{4,6},{6,8},{8,10},{10,12},{12,14},{14,16},{16,18},{18... | collective-permute-start | bytes 294920 | tf_op jit(solution)/shard_map/ppermute | solution.py:21
  14.2 6.5 %collective-permute-start.1 = (bf16[128,384]{1,0:T(8,128)(2,1)S(1)}, bf16[128,384]{1,0:T(8,128)(2,1)S(1)}, u32[]{:S(2)}, u32[]{:S(2)}) collective-permute-start(bf16[128,384]{1,0:T(8,128)(2,1)S(1)} %get-tuple-element.17), channel_id=1, source_target_pairs={{2,0},{4,2},{6,4},{8,6},{10,8},{12,10},{14,12},{16,14},{18,16},{20... | collective-permute-start | bytes 294920 | tf_op jit(solution)/shard_map/ppermute | solution.py:22
  15.6 8.7 %copy-start.6 = (f32[4]{0:T(128)S(1)}, f32[4]{0:T(128)}, u32[]{:S(2)}) copy-start(f32[4]{0:T(128)} %param.16) | copy-start | bytes 52
  26.8 2.3 copy-start.3
  26.8 2.6 copy-start.4
  29.0 102.7 %all-gather.7.cloned.1.call-start = ((), (), s32[]{:S(2)}) async-start(), calls=%async_computation.4 | async-start | bytes 7208960 | tf_op jit(solution)/shard_map/all_gather | solution.py:63
  30.7 12.8 %collective-permute-start.2 = (bf16[1,128,1408]{1,2,0:T(8,128)(2,1)}, bf16[1,128,1408]{1,2,0:T(8,128)(2,1)S(1)}, u32[]{:S(2)}, u32[]{:S(2)}) collective-permute-start(bf16[1,128,1408]{1,2,0:T(8,128)(2,1)} %get-tuple-element.10), channel_id=1, source_target_pairs={{0,24},{8,0},{16,8},{24,16},{1,25},{9,1},{17,9},{25,17},{2,26},{10... | collective-permute-start | bytes 1081352 | tf_op jit(solution)/shard_map/ppermute | solution.py:32
  34.3 29.7 %collective-permute-start.3 = (bf16[1,128,1408]{1,2,0:T(8,128)(2,1)S(1)}, bf16[1,128,1408]{1,2,0:T(8,128)(2,1)S(1)}, u32[]{:S(2)}, u32[]{:S(2)}) collective-permute-start(bf16[1,128,1408]{1,2,0:T(8,128)(2,1)S(1)} %get-tuple-element.11), channel_id=1, source_target_pairs={{0,16},{8,24},{16,0},{24,8},{1,17},{9,25},{17,1},{25,9},{2,18},{10... | collective-permute-start | bytes 1081352 | tf_op jit(solution)/shard_map/ppermute | solution.py:32
  34.3 29.8 %collective-permute-start.4 = (bf16[1,128,1408]{1,2,0:T(8,128)(2,1)S(1)}, bf16[1,128,1408]{1,2,0:T(8,128)(2,1)S(1)}, u32[]{:S(2)}, u32[]{:S(2)}) collective-permute-start(bf16[1,128,1408]{1,2,0:T(8,128)(2,1)S(1)} %get-tuple-element.9), channel_id=1, source_target_pairs={{0,8},{8,16},{16,24},{24,0},{1,9},{9,17},{17,25},{25,1},{2,10},{10... | collective-permute-start | bytes 1081352 | tf_op jit(solution)/shard_map/ppermute | solution.py:32
  64.6 3.4 copy-start.5
  66.2 131.6 %all-gather.5.cloned.1.call-start = ((), (), s32[]{:S(2)}) async-start(), calls=%async_computation.3 | async-start | bytes 7077888 | tf_op jit(solution)/shard_map/all_gather | solution.py:118
  70.7 168.9 %all-gather.9.cloned.1.call-start = ((), (), s32[]{:S(2)}) async-start(), calls=%async_computation.5 | async-start | bytes 3604480 | tf_op jit(solution)/shard_map/all_gather | solution.py:120
  72.3 8.9 %collective-permute-start.5 = (bf16[1,704,128]{2,0,1:T(2,128)(2,1)S(1)}, bf16[1,704,128]{2,0,1:T(2,128)(2,1)S(1)}, u32[]{:S(2)}, u32[]{:S(2)}) collective-permute-start(bf16[1,704,128]{2,0,1:T(2,128)(2,1)S(1)} %copy.31), channel_id=1, source_target_pairs={{0,24},{8,0},{16,8},{24,16},{1,25},{9,1},{17,9},{25,17},{2,26},{10... | collective-permute-start | bytes 540680 | tf_op jit(solution)/shard_map/ppermute | solution.py:32
  72.7 33.0 %collective-permute-start.6 = (bf16[1,704,128]{2,0,1:T(2,128)(2,1)S(1)}, bf16[1,704,128]{2,0,1:T(2,128)(2,1)S(1)}, u32[]{:S(2)}, u32[]{:S(2)}) collective-permute-start(bf16[1,704,128]{2,0,1:T(2,128)(2,1)S(1)} %copy.32), channel_id=1, source_target_pairs={{0,16},{8,24},{16,0},{24,8},{1,17},{9,25},{17,1},{25,9},{2,18},{10... | collective-permute-start | bytes 540680 | tf_op jit(solution)/shard_map/ppermute | solution.py:32
  75.5 30.9 %collective-permute-start.7 = (bf16[1,704,128]{2,0,1:T(2,128)(2,1)S(1)}, bf16[1,704,128]{2,0,1:T(2,128)(2,1)}, u32[]{:S(2)}, u32[]{:S(2)}) collective-permute-start(bf16[1,704,128]{2,0,1:T(2,128)(2,1)S(1)} %copy.33), channel_id=1, source_target_pairs={{0,8},{8,16},{16,24},{24,0},{1,9},{9,17},{17,25},{25,1},{2,10},{10... | collective-permute-start | bytes 540680 | tf_op jit(solution)/shard_map/ppermute | solution.py:32
  105.7 0.7 copy-start.2
  115.3 215.3 %reduce-scatter.5.cloned.1.call-start = ((), (), s32[]{:S(2)}) async-start(), calls=%async_computation.6 | async-start | bytes 7077888 | tf_op jit(solution)/shard_map/reduce_scatter | solution.py:128
  260.9 90.1 %all-gather.11.cloned.1.call-start = ((), (), s32[]{:S(2)}) async-start(), calls=%async_computation.7 | async-start | bytes 2359296 | tf_op jit(solution)/shard_map/all_gather | solution.py:133
  337.1 16.7 %copy-start.1 = (bf16[512,2048]{1,0:T(8,128)(2,1)S(1)}, bf16[512,2048]{1,0:T(8,128)(2,1)}, u32[]{:S(2)}) copy-start(bf16[512,2048]{1,0:T(8,128)(2,1)} %param.17) | copy-start | bytes 6291460
Sparse Core Ops, SparseCore 0:
  29.2 11.0 reduce-scatter.2
  342.6 8.3 all-gather.10
Sparse Core Ops, SparseCore 1:
  66.2 65.4 all-gather.6
  133.2 64.5 all-gather.4
  199.5 40.0 all-gather.8
  260.9 69.6 reduce-scatter.4
